TPU v7x, 32 devices: a whole 2x2x4 slice. The times are simulated.
32 devices in a mesh: fs: 8 (over z, y), tp: 4 (over x, core).
Axes of the slice: x: 2, y: 2, z: 4, core: 2. Of those that a mesh axis runs over, the one named last changes fastest.
Arguments:
- inputs: bfloat16 [16384, 2048], P('fs'), may hold values from -6 to 6
- cotangents: bfloat16 [3, 16384, 1024], P(None, 'fs', 'tp'), as said below
- factor: bfloat16 [2048, 256], P('fs'), as said below
- weights: float32 [3, 2048, 1024], P(None, 'fs', 'tp'), may hold values from -0.125 to 0.125
- first_moment: float32 [3, 256, 1024], P(None, 'fs', 'tp'), may hold values from -0.6 to 0.6
- second_moment: float32 [3, 256, 1024], P(None, 'fs', 'tp'), may hold values from 0.001 to 0.01
Outputs:
- update: float32 [3, 2048, 1024], P(None, 'fs', 'tp')
- new_weights: float32 [3, 2048, 1024], P(None, 'fs', 'tp')
- copies: bfloat16 [3, 2048, 1024], P(None, None, 'tp')
- new_first: float32 [3, 256, 1024], P(None, 'fs', 'tp')
- new_second: float32 [3, 256, 1024], P(None, 'fs', 'tp')
Inputs may be any that keep to these rules, and one draw needn't show every extreme that they name: A real-valued factor of full rank. real-valued cotangents.
All inputs are finite; a program needn't handle non-finite values.
Results may differ from a plain program's by a relative error of at most 0.0085.
Values may be sent and summed in bfloat16 or wider, within the bound.
A program may use at most 64 MiB of HBM per device.

v0:
```python
import jax
import jax.numpy as jnp
from jax import lax
from jax.sharding import PartitionSpec as P

MW = 1024
RANK = 256


def on_device(inputs, cotangents, factor, weights, first_moment, second_moment):
    factor_wide = factor.astype(jnp.float32)
    local_gradient = jnp.einsum(
        "td,mtc->dmc", inputs, cotangents, preferred_element_type=jnp.float32
    )
    gradient_high = local_gradient.astype(jnp.bfloat16)
    gradient_low = (local_gradient - gradient_high.astype(jnp.float32)).astype(jnp.bfloat16)
    factor_piece = lax.all_gather(factor, "fs", axis=0, tiled=True)
    high_term = jnp.einsum(
        "dr,dmc->rmc", factor_piece, gradient_high, preferred_element_type=jnp.float32
    )
    low_term = jnp.einsum(
        "dr,dmc->rmc", factor_piece, gradient_low, preferred_element_type=jnp.float32
    )
    partial_value = high_term + low_term
    summed = lax.psum_scatter(partial_value, "fs", scatter_dimension=0, tiled=True)
    projected = jnp.transpose(summed, (1, 0, 2))
    square_sum = lax.psum(jnp.sum(projected * projected), ("fs", "tp"))
    root_mean = jnp.sqrt(square_sum / (3 * RANK * MW) + 1e-06)
    clip_factor = jnp.minimum(1.0, 0.25 / root_mean)
    clipped = clip_factor * projected
    new_first = 0.9 * first_moment + 0.1 * clipped
    new_second = 0.95 * second_moment + 0.05 * clipped * clipped
    normed = new_first / (jnp.sqrt(new_second) + 1e-08)
    normed_whole = lax.all_gather(normed, "fs", axis=1, tiled=True)
    update = jnp.einsum("dr,mrc->mdc", factor_wide, normed_whole, precision=lax.Precision.HIGHEST)
    new_weights = weights - 0.02 * update
    copies = lax.all_gather(new_weights.astype(jnp.bfloat16), "fs", axis=1, tiled=True)
    return (update, new_weights, copies, new_first, new_second)


def solution(mesh):
    placed = (
        P("fs", None),
        P(None, "fs", "tp"),
        P("fs", None),
        P(None, "fs", "tp"),
        P(None, "fs", "tp"),
        P(None, "fs", "tp"),
    )
    return jax.shard_map(
        on_device,
        mesh=mesh,
        in_specs=placed,
        out_specs=(
            P(None, "fs", "tp"),
            P(None, "fs", "tp"),
            P(None, None, "tp"),
            P(None, "fs", "tp"),
            P(None, "fs", "tp"),
        ),
        check_vma=False,
    )
```

profile of v0, /device:TPU:0, one launch (start us, length us, event | category | flops | bytes accessed | tf_op | source)
XLA Modules:
  0.0 294.2 jit_solution(1546172498071317333)
XLA Ops:
  7.2 0.0 copy-start
  7.2 0.0 all-gather.3.cloned.1.call-start
  7.2 0.7 all-gather.3.cloned.1.call-update
  7.9 0.0 all-reduce.3.cloned.1.call-start
  8.0 1.1 copy-done
  9.1 10.9 %fusion = f32[2048,3,256]{2,0,1:T(8,128)} fusion(bf16[3,2048,256]{2,1,0:T(8,128)(2,1)S(1)} %copy-done, bf16[2048,2048]{1,0:T(8,128)(2,1)} %param.6), kind=kOutput, calls=%fused_computation | convolution fusion | flops 6442450944 | bytes 17825792 | tf_op jit(solution)/shard_map/td,mtc->dmc/dot_general | solution.py:12
  19.9 33.2 %all-gather.3.cloned.1.call-done = bf16[2048,256]{1,0:T(8,128)(2,1)} async-done(((bf16[256,256]{1,0:T(8,128)(2,1)}), bf16[2048,256]{1,0:T(8,128)(2,1)}) %all-gather.3.cloned.1.call-update) | async-done | bytes 1048592 | tf_op jit(solution)/shard_map/all_gather | solution.py:17
  53.1 0.0 copy-start.1
  53.2 0.0 copy-start.2
  53.2 6.0 %fusion.2 = f32[3,256,256]{2,1,0:T(8,128)S(1)} fusion(f32[2048,3,256]{2,0,1:T(8,128)} %fusion, bf16[2048,256]{1,0:T(8,128)(2,1)} %all-gather.3.cloned.1.call-done), kind=kOutput, calls=%fused_computation.3 | convolution fusion | flops 811597824 | bytes 8126464 | tf_op jit(solution)/shard_map/dr,dmc->rmc/dot_general | solution.py:21
  59.2 0.6 copy-done.1
  59.8 0.3 copy-done.2
  60.1 0.0 copy-start.5
  60.1 0.0 copy-start.4
  60.1 0.0 copy-start.3
  60.1 1.9 fusion.9
  62.0 2.4 copy.39
  64.4 0.0 all-reduce.3.cloned.1.call-update
  64.5 0.0 all-gather.5.cloned.1.call-start
  64.5 0.0 copy-done.5
  64.5 0.6 dynamic-slice
  65.8 2.3 copy.41
  68.0 73.6 %all-reduce.3.cloned.1.call-done = f32[256,3,256]{2,1,0:T(4,128)} async-done(((f32[256,3,256]{2,1,0:T(4,128)}), f32[256,3,256]{2,1,0:T(4,128)}) %all-reduce.3.cloned.1.call-update) | async-done | bytes 786448
  141.6 1.6 multiply_reduce_fusion
  143.2 39.7 %psum.7 = f32[]{:T(128)} all-reduce(f32[]{:T(128)} %get-tuple-element.25), channel_id=1, replica_groups=mesh['fs'=8,'tp'=4] {'fs','tp'}, use_global_device_ids=true, to_apply=%region_2.0 | all-reduce | flops 1 | bytes 8 | tf_op jit(solution)/shard_map/psum | solution.py:27
  183.7 0.0 copy-done.4
  183.7 1.6 add_divide_fusion
  185.3 32.0 %all_gather.10 = f32[3,256,256]{2,1,0:T(8,128)S(1)} all-gather(f32[3,32,256]{2,1,0:T(8,128)S(1)} %get-tuple-element.22), channel_id=1, replica_groups=mesh['fs'=8,'tp'=4] {'fs'}, dimensions={1}, use_global_device_ids=true | all-gather | bytes 884736 | tf_op jit(solution)/shard_map/all_gather | solution.py:34
  217.3 0.0 copy-done.3
  217.3 3.2 %fusion.17 = (bf16[3,256,256]{1,2,0:T(8,128)(2,1)}, f32[3,256,256]{1,2,0:T(8,128)}, f32[3,256,256]{1,2,0:T(8,128)}) fusion(f32[3,256,256]{1,2,0:T(8,128)} %copy.41, f32[3,256,256]{2,1,0:T(8,128)S(1)} %all_gather.10, bf16[256,256]{1,0:T(8,128)(2,1)S(1)} %copy-done.3), kind=kOutput, calls=%fused_computation.22 | convolution fusion | flops 604569600 | bytes 3670016 | tf_op jit(solution)/shard_map/dr,mrc->mdc/dot_general | solution.py:35
  220.5 0.0 all-gather.5.cloned.1.call-update
  220.5 2.3 copy.42
  222.8 2.3 copy.43
  225.1 57.9 %all-gather.5.cloned.1.call-done = bf16[3,2048,256]{1,2,0:T(8,128)(2,1)} async-done(((bf16[3,256,256]{1,2,0:T(8,128)(2,1)}), bf16[3,2048,256]{1,2,0:T(8,128)(2,1)}) %all-gather.5.cloned.1.call-update) | async-done | bytes 3145744 | tf_op jit(solution)/shard_map/all_gather | solution.py:37
  283.0 4.6 %copy.44 = bf16[3,2048,256]{2,1,0:T(8,128)(2,1)} copy(bf16[3,2048,256]{1,2,0:T(8,128)(2,1)} %all-gather.5.cloned.1.call-done) | data formatting | bytes 6291456
Async XLA Ops:
  7.2 1.9 copy-start
  7.2 46.0 %all-gather.3.cloned.1.call-start = ((), (), s32[]{:S(2)}) async-start(), calls=%async_computation | async-start | bytes 1179648 | tf_op jit(solution)/shard_map/all_gather | solution.py:17
  7.9 133.7 %all-reduce.3.cloned.1.call-start = ((), (), s32[]{:S(2)}) async-start(), calls=%async_computation.2 | async-start | bytes 2097152
  53.1 6.7 %copy-start.1 = (f32[2048,3,256]{2,0,1:T(8,128)S(1)}, f32[2048,3,256]{2,0,1:T(8,128)}, u32[]{:S(2)}) copy-start(f32[2048,3,256]{2,0,1:T(8,128)} %fusion) | copy-start | bytes 18874372
  53.2 6.9 %copy-start.2 = (bf16[2048,256]{1,0:T(8,128)(2,1)S(1)}, bf16[2048,256]{1,0:T(8,128)(2,1)}, u32[]{:S(2)}) copy-start(bf16[2048,256]{1,0:T(8,128)(2,1)} %all-gather.3.cloned.1.call-done) | copy-start | bytes 3145732
  60.1 4.4 %copy-start.5 = (u32[32]{0:T(128)S(1)}, u32[32]{0:T(128)}, u32[]{:S(2)}) copy-start(u32[32]{0:T(128)} %constant.25) | copy-start | bytes 388
  60.1 123.6 %copy-start.4 = (f32[3,32,256]{2,1,0:T(8,128)S(1)}, f32[3,32,256]{2,1,0:T(8,128)}, u32[]{:S(2)}) copy-start(f32[3,32,256]{2,1,0:T(8,128)} %param.11) | copy-start | bytes 294916
  60.1 157.2 %copy-start.3 = (bf16[256,256]{1,0:T(8,128)(2,1)S(1)}, bf16[256,256]{1,0:T(8,128)(2,1)}, u32[]{:S(2)}) copy-start(bf16[256,256]{1,0:T(8,128)(2,1)} %param.8) | copy-start | bytes 393220
  64.5 218.6 %all-gather.5.cloned.1.call-start = ((), (), s32[]{:S(2)}) async-start(), calls=%async_computation.1 | async-start | bytes 3538944 | tf_op jit(solution)/shard_map/all_gather | solution.py:37
Sparse Core Ops, SparseCore 0:
  10.1 42.9 all-gather.2
  64.6 77.0 all-reduce.2
  220.7 62.2 all-gather.4
where the time goes:
time: 295 us; the launch traced here: 294 us
  waiting for transfers between devices  165 us (56%)
  blocking collectives  71.8 us (24%)
  matrix products  22 us (7%)
  local copies, waits for them, and re-layouts  16.5 us (6%)
  between operations  15.1 us (5%)
  other arithmetic  3.21 us (1%)
    unnamed x4, waiting for transfers between devices  74.3 us
    all_gather x1, waiting for transfers between devices, on_device(): lax.all_gather(new_weights.astype(jnp.bfloat16), 'fs', axis=1, tiled=True)  57.9 us
    psum x1, blocking collectives, on_device(): square_sum = lax.psum(jnp.sum(projected * projected), ('fs', 'tp'))  39.7 us
    all_gather x1, waiting for transfers between devices, on_device(): factor_piece = lax.all_gather(factor, 'fs', axis=0, tiled=True)  33.2 us
    all_gather x1, blocking collectives, on_device(): normed_whole = lax.all_gather(normed, 'fs', axis=1, tiled=True)  32 us
    unnamed x17, local copies, waits for them, and re-layouts  14.1 us
    dot_general x1, matrix products, on_device(): jnp.einsum('td,mtc->dmc', inputs, cotangents, preferred_element_type=jnp....  10.9 us
    dot_general x1, matrix products, on_device(): jnp.einsum('dr,dmc->rmc', factor_piece, gradient_low, preferred_element_t...  6.04 us
  transfers between devices with their start and end apart: 3, of which 3 were waited for; matrix products, arithmetic and copies ran while one was open for 6% of the time, Pallas kernels for 0%

commit v1 on v0

v1 whole, which is shorter than its diff:
```python
import functools

import jax
import jax.numpy as jnp
from jax import lax
from jax.experimental import pallas as pl
from jax.experimental.pallas import tpu as pltpu
from jax.sharding import PartitionSpec as P

MESH = pl.DeviceIdType.MESH


def flip(index, bits, count):
    result, weight = 0, 1
    while weight < count:
        bit = (bits // weight) % 2
        result = result + lax.rem(lax.div(index, weight) + bit, 2) * weight
        weight *= 2
    return result


def exchange_kernel(
    nfs, ntp, scale_count,
    x_hbm, c_hbm, f_ref, first_in, second_in,
    first_ref, second_ref, f_out, normed_out,
    xbuf, cbuf, pacc, fbuf, pbuf, rbuf, nbuf, sq_own, sq_tp, sq_mid, sq_fs,
    x_sem, c_sem, fo_sem,
    f_send, f_recv, d_send, d_recv, p_send, p_recv,
    t_send, t_recv, s_send, s_recv, n_send, n_recv,
):
    me, col = lax.axis_index("fs"), lax.axis_index("tp")
    core = lax.rem(col, 2)
    mate = flip(col, 1, ntp)
    chunks, chunk = xbuf.shape[0], xbuf.shape[1]
    rows = first_in.shape[1]
    peers = [flip(me, o, nfs) for o in range(1, nfs)]
    sides = [flip(col, o, ntp) for o in range(1, ntp)]

    def remote(src, dst, send, recv, fs, tp):
        return pltpu.make_async_remote_copy(
            src_ref=src, dst_ref=dst, send_sem=send, recv_sem=recv,
            device_id=(fs, tp), device_id_type=MESH,
        )

    x_copies = [
        pltpu.make_async_copy(x_hbm.at[i], xbuf.at[i], x_sem.at[i]) for i in range(chunks)
    ]
    c_copies = [pltpu.make_async_copy(c_hbm.at[m], cbuf.at[m], c_sem.at[m]) for m in range(3)]
    for copy in x_copies + c_copies:
        copy.start()

    barrier = pltpu.get_barrier_semaphore()
    for peer in peers:
        pl.semaphore_signal(barrier, inc=1, device_id=(peer, col), device_id_type=MESH)
    for side in sides:
        pl.semaphore_signal(barrier, inc=1, device_id=(me, side), device_id_type=MESH)
    pl.semaphore_wait(barrier, nfs - 1 + ntp - 1)

    sends = []
    for o, peer in enumerate(peers):
        copy = remote(f_ref.at[core], fbuf.at[me, core], f_send.at[o], f_recv.at[me], peer, col)
        copy.start()
        sends.append(copy)
    fbuf[me] = f_ref[...]
    for o, peer in enumerate(peers):
        remote(
            f_ref.at[core], fbuf.at[peer, core], f_send.at[o], f_recv.at[peer], peer, col
        ).wait_recv()
        copy = remote(
            fbuf.at[peer, core], fbuf.at[peer, core], d_send.at[o], d_recv.at[peer], me, mate
        )
        copy.start()
        sends.append(copy)
    for copy in x_copies + c_copies:
        copy.wait()
    for o, peer in enumerate(peers):
        remote(
            f_ref.at[core], fbuf.at[peer, 1 - core], d_send.at[o], d_recv.at[peer], me, mate
        ).wait_recv()
    f_copy = pltpu.make_async_copy(fbuf, f_out, fo_sem)
    f_copy.start()

    pacc[...] = jnp.zeros_like(pacc)
    whole = fbuf.shape[0] * fbuf.shape[1] * fbuf.shape[2]

    @pl.loop(0, chunks)
    def _(i):
        factor = fbuf[...].reshape(whole, fbuf.shape[3])
        low = jnp.dot(xbuf[i], factor, preferred_element_type=jnp.float32).astype(jnp.bfloat16)
        for m in range(3):
            tokens = pl.ds(pl.multiple_of(i * chunk, chunk), chunk)
            pacc[m] += lax.dot_general(
                low, cbuf[m, tokens, :], (((0,), (0,)), ((), ())),
                preferred_element_type=jnp.float32,
            )

    for m in range(3):
        for j in range(nfs):
            pbuf[j, m] = pacc[m, j * rows:(j + 1) * rows, :].astype(jnp.bfloat16)
    for o, peer in enumerate(peers):
        copy = remote(pbuf.at[peer], rbuf.at[me], p_send.at[o], p_recv.at[me], peer, col)
        copy.start()
        sends.append(copy)
    projected = pacc[:, pl.ds(pl.multiple_of(me * rows, rows), rows), :]
    for o, peer in enumerate(peers):
        remote(
            pbuf.at[peer], rbuf.at[peer], p_send.at[o], p_recv.at[peer], peer, col
        ).wait_recv()
        projected = projected + rbuf[peer].astype(jnp.float32)

    def spread(value):
        total = jnp.sum(jnp.sum(value, axis=0), axis=0, keepdims=True)
        return jnp.broadcast_to(jnp.sum(total, axis=1, keepdims=True), sq_own.shape)

    own = spread(projected * projected)
    sq_own[...] = own
    sq_tp[col] = own
    for o, side in enumerate(sides):
        copy = remote(sq_own, sq_tp.at[col], t_send.at[o], t_recv.at[col], me, side)
        copy.start()
        sends.append(copy)
    for o, side in enumerate(sides):
        remote(sq_own, sq_tp.at[side], t_send.at[o], t_recv.at[side], me, side).wait_recv()
    mid = jnp.sum(sq_tp[...], axis=0)
    sq_mid[...] = mid
    sq_fs[me] = mid
    for o, peer in enumerate(peers):
        copy = remote(sq_mid, sq_fs.at[me], s_send.at[o], s_recv.at[me], peer, col)
        copy.start()
        sends.append(copy)
    for o, peer in enumerate(peers):
        remote(sq_mid, sq_fs.at[peer], s_send.at[o], s_recv.at[peer], peer, col).wait_recv()
    square_sum = jnp.sum(sq_fs[...], axis=0)[:, :1]

    root_mean = jnp.sqrt(square_sum / scale_count + 1e-06)
    clip_factor = jnp.minimum(1.0, 0.25 / root_mean)
    clipped = clip_factor * projected
    new_first = 0.9 * first_in[...] + 0.1 * clipped
    new_second = 0.95 * second_in[...] + 0.05 * clipped * clipped
    normed = new_first / (jnp.sqrt(new_second) + 1e-08)
    nbuf[me] = normed.astype(jnp.bfloat16)
    for o, peer in enumerate(peers):
        copy = remote(nbuf.at[me], nbuf.at[me], n_send.at[o], n_recv.at[me], peer, col)
        copy.start()
        sends.append(copy)
    first_ref[...] = new_first
    second_ref[...] = new_second
    for o, peer in enumerate(peers):
        remote(
            nbuf.at[peer], nbuf.at[peer], n_send.at[o], n_recv.at[peer], peer, col
        ).wait_recv()
    for m in range(3):
        normed_out[m] = jnp.concatenate(
            [nbuf[j, m].astype(jnp.float32) for j in range(nfs)], axis=0
        ).astype(jnp.bfloat16)
    f_copy.wait()
    for copy in sends:
        copy.wait_send()


def finish_kernel(f_ref, f_all, normed, weights, gathered, update, new_weights, copies):
    step = jnp.dot(f_ref[...], normed[0], preferred_element_type=jnp.float32)
    update[0] = step
    new_weights[0] = weights[0] - 0.02 * step
    held = gathered.shape[2]
    for j in range(gathered.shape[0]):
        step = jnp.dot(f_all[j], normed[0], preferred_element_type=jnp.float32)
        copies[0, j * held:(j + 1) * held] = (
            gathered[j, 0].astype(jnp.float32) - 0.02 * step
        ).astype(jnp.bfloat16)


def on_device(nfs, ntp, inputs, cotangents, factor, weights, first_moment, second_moment):
    tokens, width = inputs.shape
    held, rank = factor.shape
    rows, cols = first_moment.shape[1:]
    chunk = min(512, tokens)
    chunks = tokens // chunk
    gathered = lax.all_gather(weights.astype(jnp.bfloat16), "fs", axis=0)

    dma = pltpu.SemaphoreType.DMA
    vmem = pl.BlockSpec(memory_space=pltpu.VMEM)
    hbm = pl.BlockSpec(memory_space=pl.ANY)
    new_first, new_second, f_all, normed = pl.pallas_call(
        functools.partial(exchange_kernel, nfs, ntp, 3 * rank * cols * ntp),
        out_shape=(
            jax.ShapeDtypeStruct(first_moment.shape, jnp.float32),
            jax.ShapeDtypeStruct(second_moment.shape, jnp.float32),
            jax.ShapeDtypeStruct((nfs, 2, held // 2, rank), jnp.bfloat16),
            jax.ShapeDtypeStruct((3, rank, cols), jnp.bfloat16),
        ),
        in_specs=[hbm, hbm, vmem, vmem, vmem],
        out_specs=(vmem, vmem, hbm, vmem),
        scratch_shapes=[
            pltpu.VMEM((chunks, chunk, width), jnp.bfloat16),
            pltpu.VMEM(cotangents.shape, jnp.bfloat16),
            pltpu.VMEM((3, rank, cols), jnp.float32),
            pltpu.VMEM((nfs, 2, held // 2, rank), jnp.bfloat16),
            pltpu.VMEM((nfs, 3, rows, cols), jnp.bfloat16),
            pltpu.VMEM((nfs, 3, rows, cols), jnp.bfloat16),
            pltpu.VMEM((nfs, 3, rows, cols), jnp.bfloat16),
            pltpu.VMEM((1, 128), jnp.float32),
            pltpu.VMEM((ntp, 1, 128), jnp.float32),
            pltpu.VMEM((1, 128), jnp.float32),
            pltpu.VMEM((nfs, 1, 128), jnp.float32),
            dma((chunks,)), dma((3,)), dma,
            dma((nfs,)), dma((nfs,)), dma((nfs,)), dma((nfs,)), dma((nfs,)), dma((nfs,)),
            dma((ntp,)), dma((ntp,)), dma((nfs,)), dma((nfs,)), dma((nfs,)), dma((nfs,)),
        ],
        compiler_params=pltpu.CompilerParams(
            collective_id=0, has_side_effects=True, vmem_limit_bytes=63 * 2**20
        ),
        cost_estimate=pl.CostEstimate(
            flops=50_000_000_000, bytes_accessed=100_000_000, transcendentals=0
        ),
        name="exchange",
    )(
        inputs.reshape(chunks, chunk, width), cotangents,
        factor.reshape(2, held // 2, rank), first_moment, second_moment,
    )
    f_all = f_all.reshape(nfs, held, rank)
    update, new_weights, copies = pl.pallas_call(
        finish_kernel,
        grid=(3,),
        out_shape=(
            jax.ShapeDtypeStruct(weights.shape, jnp.float32),
            jax.ShapeDtypeStruct(weights.shape, jnp.float32),
            jax.ShapeDtypeStruct((3, nfs * held, cols), jnp.bfloat16),
        ),
        in_specs=[
            pl.BlockSpec((held, rank), lambda m: (0, 0)),
            pl.BlockSpec((nfs, held, rank), lambda m: (0, 0, 0)),
            pl.BlockSpec((1, rank, cols), lambda m: (m, 0, 0)),
            pl.BlockSpec((1, held, cols), lambda m: (m, 0, 0)),
            pl.BlockSpec((nfs, 1, held, cols), lambda m: (0, m, 0, 0)),
        ],
        out_specs=(
            pl.BlockSpec((1, held, cols), lambda m: (m, 0, 0)),
            pl.BlockSpec((1, held, cols), lambda m: (m, 0, 0)),
            pl.BlockSpec((1, nfs * held, cols), lambda m: (m, 0, 0)),
        ),
        name="finish",
    )(factor, f_all, normed, weights, gathered)
    return (update, new_weights, copies, new_first, new_second)


def solution(mesh):
    placed = (
        P("fs", None),
        P(None, "fs", "tp"),
        P("fs", None),
        P(None, "fs", "tp"),
        P(None, "fs", "tp"),
        P(None, "fs", "tp"),
    )
    return jax.shard_map(
        functools.partial(on_device, mesh.shape["fs"], mesh.shape["tp"]),
        mesh=mesh,
        in_specs=placed,
        out_specs=(
            P(None, "fs", "tp"),
            P(None, "fs", "tp"),
            P(None, None, "tp"),
            P(None, "fs", "tp"),
            P(None, "fs", "tp"),
        ),
        check_vma=False,
    )
```

time: 295 us -> 101 us (0.34)
  waiting for transfers between devices: 165 us -> 8.63 us
  Pallas kernels: 0 us -> 74.5 us
  blocking collectives: 71.8 us -> 0 us
  matrix products: 22 us -> 0 us
  local copies, waits for them, and re-layouts: 16.5 us -> 1.29 us
    all_gather x2 -> x1, waiting for transfers between devices: 91.1 us -> 8.61 us  [on_device(): gathered = lax.all_gather(weights.astype(jnp.bfloat16), 'fs', axis=0)]
    pallas_call x0 -> x2, Pallas kernels: none -> 74.5 us  [the longest x1 68.5 us: on_device(): pl.pallas_call(functools.partial(exchange_kernel, nfs, ntp, 3 * rank * co...]
    unnamed x4 -> x1, waiting for transfers between devices: 74.3 us -> 0.02 us
    psum x1 -> x0, blocking collectives: 39.7 us -> none  [on_device(): square_sum = lax.psum(jnp.sum(projected * projected), ('fs', 'tp'))]
    all_gather x1 -> x0, blocking collectives: 32 us -> none  [on_device(): normed_whole = lax.all_gather(normed, 'fs', axis=1, tiled=True)]
    dot_general x4 -> x0, matrix products: 22 us -> none  [the longest x1 10.9 us: on_device(): jnp.einsum('td,mtc->dmc', inputs, cotangents, preferred_element_type=jnp....]
    unnamed x17 -> x6, local copies, waits for them, and re-layouts: 14.1 us -> 1.29 us
  transfers between devices with their start and end apart: 3 -> 1, of which waited for: 3 -> 1; matrix products, arithmetic and copies ran while one was open for 6% -> 0% of each run, Pallas kernels for 0% -> 68%
where the time goes in v1:
time: 101 us; the launch traced here: 100 us
  Pallas kernels  74.5 us (74%)
  between operations  14.1 us (14%)
  waiting for transfers between devices  8.63 us (9%)
  other arithmetic  1.92 us (2%)
  local copies, waits for them, and re-layouts  1.29 us (1%)
    pallas_call x1, Pallas kernels, on_device(): pl.pallas_call(functools.partial(exchange_kernel, nfs, ntp, 3 * rank * co...  68.5 us
    all_gather x1, waiting for transfers between devices, on_device(): gathered = lax.all_gather(weights.astype(jnp.bfloat16), 'fs', axis=0)  8.61 us
    pallas_call x1, Pallas kernels, on_device(): pl.pallas_call(finish_kernel, grid=(3,), out_shape=(jax.ShapeDtypeStruct(...  6.01 us
  transfers between devices with their start and end apart: 1, of which 1 were waited for; matrix products, arithmetic and copies ran while one was open for 0% of the time, Pallas kernels for 68%

profile of v1, /device:TPU:0, one launch (start us, length us, event | category | flops | bytes accessed | tf_op | source)
XLA Modules:
  0.0 100.4 jit_solution(2362917567093380516)
XLA Ops:
  7.2 0.0 all-gather.3.cloned.1.call-start
  7.2 1.9 %convert_element_type.3 = bf16[3,256,256]{2,1,0:T(8,128)(2,1)} convert(f32[3,256,256]{2,1,0:T(8,128)} %weights.1) | non-fusion elementwise | flops 196608 | bytes 1179648 | tf_op jit(solution)/shard_map/convert_element_type | solution.py:179
  9.1 0.0 all-gather.3.cloned.1.call-update
  9.2 68.5 %exchange.1 = (f32[3,32,256]{2,1,0:T(8,128)}, f32[3,32,256]{2,1,0:T(8,128)}, bf16[8,2,128,256]{3,2,1,0:T(8,128)(2,1)}, bf16[3,256,256]{2,1,0:T(8,128)(2,1)}) custom-call(bf16[4,512,2048]{2,1,0:T(8,128)(2,1)} %bitcast.7, bf16[3,2048,256]{2,1,0:T(8,128)(2,1)} %c_hbm.1, bf16[2,128,256]{2,1,0:T(8,128)(2,1)} %bitcast.6, f32[3,32,256]{2,1,0:T(8,128)} %first_in.1, ...), custom_call_target="tpu_custom_call" | custom-call | flops 49999998976 | bytes 100000000 | tf_op jit(solution)/shard_map/exchange/pallas_call | solution.py:184
  77.6 0.0 copy-start.1
  77.7 0.0 copy-start
  77.7 8.6 %all-gather.3.cloned.1.call-done = bf16[24,256,256]{2,1,0:T(8,128)(2,1)} async-done(((bf16[3,256,256]{2,1,0:T(8,128)(2,1)}), bf16[24,256,256]{2,1,0:T(8,128)(2,1)}) %all-gather.3.cloned.1.call-update) | async-done | bytes 3145744 | tf_op jit(solution)/shard_map/all_gather | solution.py:179
  86.3 6.0 %finish.1 = (f32[3,256,256]{2,1,0:T(8,128)}, f32[3,256,256]{2,1,0:T(8,128)}, bf16[3,2048,256]{2,1,0:T(8,128)(2,1)}) custom-call(bf16[256,256]{1,0:T(8,128)(2,1)} %f_ref.1, bf16[8,256,256]{2,1,0:T(8,128)(2,1)} %bitcast.5, bf16[3,256,256]{2,1,0:T(8,128)(2,1)} %get-tuple-element.13.normed, f32[3,256,256]{2,1,0:T(8,128)} %weights.1, bf16[8,3,256,256]{3,2,1,0:T(8,128)(2,1)} %bitcast.4), custom_call_target="tpu_custom_call" | custom-call | tf_op jit(solution)/shard_map/finish/pallas_call | solution.py:222
  92.3 0.0 copy-done.1
  92.3 0.6 copy.13
  92.9 0.0 copy-done
  92.9 0.6 copy.14
Async XLA Ops:
  7.2 79.1 %all-gather.3.cloned.1.call-start = ((), (), s32[]{:S(2)}) async-start(), calls=%async_computation | async-start | bytes 3538944 | tf_op jit(solution)/shard_map/all_gather | solution.py:179
  77.6 14.7 %copy-start.1 = (f32[3,32,256]{2,1,0:T(8,128)S(1)}, f32[3,32,256]{2,1,0:T(8,128)}, u32[]{:S(2)}) copy-start(f32[3,32,256]{2,1,0:T(8,128)} %get-tuple-element.27) | copy-start | bytes 294916
  77.7 15.3 %copy-start = (f32[3,32,256]{2,1,0:T(8,128)S(1)}, f32[3,32,256]{2,1,0:T(8,128)}, u32[]{:S(2)}) copy-start(f32[3,32,256]{2,1,0:T(8,128)} %get-tuple-element.28) | copy-start | bytes 294916
Sparse Core Ops, SparseCore 0:
  10.7 75.4 all-gather.2

commit v2 on v1

v2 whole, which is shorter than its diff:
```python
import functools

import jax
import jax.numpy as jnp
from jax import lax
from jax.experimental import pallas as pl
from jax.experimental.pallas import tpu as pltpu
from jax.sharding import PartitionSpec as P

MESH = pl.DeviceIdType.MESH


def flip(index, bits, count):
    result, weight = 0, 1
    while weight < count:
        bit = (bits // weight) % 2
        result = result + lax.rem(lax.div(index, weight) + bit, 2) * weight
        weight *= 2
    return result


def ring_index(place, count):
    place = lax.rem(place + count, count)
    odd = lax.div(place, count // 2)
    return (1 - odd) * 2 * place + odd * (2 * (count - 1 - place) + 1)


def exchange_kernel(
    nfs, ntp, scale_count,
    x_hbm, c_hbm, f_hbm, w_hbm, first_hbm, second_hbm,
    first_ref, second_ref, f_out, normed_out, w_out,
    xbuf, cbuf, wide, first_in, second_in,
    pacc, fbuf, wbuf, pbuf, rbuf, nbuf, sq_own, sq_tp, sq_mid, sq_fs,
    x_sem, c_sem, in_sem, fo_sem, wo_sem,
    f_send, f_recv, d_send, d_recv, w_send, w_recv, p_send, p_recv,
    t_send, t_recv, s_send, s_recv, n_send, n_recv,
):
    me, col = lax.axis_index("fs"), lax.axis_index("tp")
    core = lax.rem(col, 2)
    mate = flip(col, 1, ntp)
    chunks, chunk = xbuf.shape[0], xbuf.shape[1]
    rows = first_in.shape[1]
    half = wbuf.shape[3]
    peers = [flip(me, o, nfs) for o in range(1, nfs)]
    sides = [flip(col, o, ntp) for o in range(1, ntp)]
    odd = lax.rem(me, 2)
    place = (1 - odd) * lax.div(me, 2) + odd * (nfs - 1 - lax.div(me, 2))
    onward = [ring_index(place + 1, nfs), ring_index(place - 1, nfs)]
    hops = [nfs // 2, (nfs - 1) // 2]
    sends = []

    def origin(way, step):
        return ring_index(place - step if way == 0 else place + step, nfs)

    def remote(src, dst, send, recv, fs, tp):
        return pltpu.make_async_remote_copy(
            src_ref=src, dst_ref=dst, send_sem=send, recv_sem=recv,
            device_id=(fs, tp), device_id_type=MESH,
        )

    def begin(copy):
        copy.start()
        sends.append(copy)

    f_copy = pltpu.make_async_copy(f_hbm, fbuf.at[me], in_sem.at[0])
    w_copy = pltpu.make_async_copy(w_hbm, wide, in_sem.at[1])
    moments = [
        pltpu.make_async_copy(first_hbm, first_in, in_sem.at[2]),
        pltpu.make_async_copy(second_hbm, second_in, in_sem.at[3]),
    ]
    x_copies = [
        pltpu.make_async_copy(x_hbm.at[i], xbuf.at[i], x_sem.at[i]) for i in range(chunks)
    ]
    c_copies = [pltpu.make_async_copy(c_hbm.at[m], cbuf.at[m], c_sem.at[m]) for m in range(3)]
    for copy in [f_copy, w_copy] + x_copies + c_copies + moments:
        copy.start()

    barrier = pltpu.get_barrier_semaphore()
    for peer in peers:
        pl.semaphore_signal(barrier, inc=1, device_id=(peer, col), device_id_type=MESH)
    for side in sides:
        pl.semaphore_signal(barrier, inc=1, device_id=(me, side), device_id_type=MESH)
    f_copy.wait()
    w_copy.wait()
    for way in range(2):
        for m in range(3):
            wbuf[me, way, m] = wide[m, way * half:(way + 1) * half, :].astype(jnp.bfloat16)
    pl.semaphore_wait(barrier, nfs - 1 + ntp - 1)

    def pass_weights(way, step, m):
        held = wbuf.at[origin(way, step), way, m]
        return remote(
            held, held, w_send.at[way, m, step], w_recv.at[way, m, origin(way, step)],
            onward[way], col,
        )

    stores = []

    def store_weights(way, step):
        where = origin(way, step)
        copy = pltpu.make_async_copy(
            wbuf.at[where, way], w_out.at[where, way], wo_sem.at[way, step]
        )
        copy.start()
        stores.append(copy)

    ticks = [(step, m) for step in range(1, nfs) for m in range(3)]
    total_ticks = len(ticks)

    def advance(part):
        while ticks and (total_ticks - len(ticks)) * 21 < part * total_ticks:
            step, m = ticks.pop(0)
            for way in range(2):
                pass_weights(way, step, m).wait_recv()
                if step < nfs - 1:
                    begin(pass_weights(way, step, m))
                if m == 2:
                    store_weights(way, step)

    def pass_factor(way, step):
        held = fbuf.at[origin(way, step), core]
        return remote(
            held, held, f_send.at[way, step], f_recv.at[origin(way, step)], onward[way], col
        )

    def share_factor(way, step, which):
        held = fbuf.at[origin(way, step), which]
        return remote(
            held, held, d_send.at[way, step], d_recv.at[origin(way, step)], me, mate
        )

    for way in range(2):
        begin(pass_factor(way, 0))
    for step in range(1, hops[0] + 1):
        for way in range(2):
            if step <= hops[way]:
                pass_factor(way, step).wait_recv()
                if step < hops[way]:
                    begin(pass_factor(way, step))
                begin(share_factor(way, step, core))
        if step <= 3:
            for way in range(2):
                begin(pass_weights(way, 0, step - 1))
                if step == 3:
                    store_weights(way, 0)
    for copy in x_copies + c_copies:
        copy.wait()
    for way in range(2):
        for step in range(1, hops[way] + 1):
            share_factor(way, step, 1 - core).wait_recv()
    fo_copy = pltpu.make_async_copy(fbuf, f_out, fo_sem)
    fo_copy.start()

    pacc[...] = jnp.zeros_like(pacc)
    whole = fbuf.shape[0] * fbuf.shape[1] * fbuf.shape[2]
    for i in range(chunks):
        factor = fbuf[...].reshape(whole, fbuf.shape[3])
        low = jnp.dot(xbuf[i], factor, preferred_element_type=jnp.float32).astype(jnp.bfloat16)
        for m in range(3):
            pacc[m] += lax.dot_general(
                low, cbuf[m, i * chunk:(i + 1) * chunk, :], (((0,), (0,)), ((), ())),
                preferred_element_type=jnp.float32,
            )
        if i < chunks - 1:
            advance(i + 1)

    for m in range(3):
        for j in range(nfs):
            pbuf[j, m] = pacc[m, j * rows:(j + 1) * rows, :].astype(jnp.bfloat16)
    for o, peer in enumerate(peers):
        begin(remote(pbuf.at[peer], rbuf.at[me], p_send.at[o], p_recv.at[me], peer, col))
    projected = pacc[:, pl.ds(pl.multiple_of(me * rows, rows), rows), :]
    for o, peer in enumerate(peers):
        advance(4 + (o * 6) // len(peers))
        remote(
            pbuf.at[peer], rbuf.at[peer], p_send.at[o], p_recv.at[peer], peer, col
        ).wait_recv()
        projected = projected + rbuf[peer].astype(jnp.float32)

    def spread(value):
        total = jnp.sum(jnp.sum(value, axis=0), axis=0, keepdims=True)
        return jnp.broadcast_to(jnp.sum(total, axis=1, keepdims=True), sq_own.shape)

    own = spread(projected * projected)
    sq_own[...] = own
    sq_tp[col] = own
    for o, side in enumerate(sides):
        begin(remote(sq_own, sq_tp.at[col], t_send.at[o], t_recv.at[col], me, side))
    advance(11)
    for o, side in enumerate(sides):
        remote(sq_own, sq_tp.at[side], t_send.at[o], t_recv.at[side], me, side).wait_recv()
    mid = jnp.sum(sq_tp[...], axis=0)
    sq_mid[...] = mid
    sq_fs[me] = mid
    for o, peer in enumerate(peers):
        begin(remote(sq_mid, sq_fs.at[me], s_send.at[o], s_recv.at[me], peer, col))
    for copy in moments:
        copy.wait()
    advance(13)
    for o, peer in enumerate(peers):
        remote(sq_mid, sq_fs.at[peer], s_send.at[o], s_recv.at[peer], peer, col).wait_recv()
    square_sum = jnp.sum(sq_fs[...], axis=0)[:, :1]

    root_mean = jnp.sqrt(square_sum / scale_count + 1e-06)
    clip_factor = jnp.minimum(1.0, 0.25 / root_mean)
    clipped = clip_factor * projected
    new_first = 0.9 * first_in[...] + 0.1 * clipped
    new_second = 0.95 * second_in[...] + 0.05 * clipped * clipped
    normed = new_first / (jnp.sqrt(new_second) + 1e-08)
    nbuf[me] = normed.astype(jnp.bfloat16)

    def pass_normed(way, step):
        held = nbuf.at[origin(way, step)]
        return remote(
            held, held, n_send.at[way, step], n_recv.at[origin(way, step)], onward[way], col
        )

    for way in range(2):
        begin(pass_normed(way, 0))
    first_ref[...] = new_first
    second_ref[...] = new_second
    for step in range(1, hops[0] + 1):
        advance(13 + (step * 7) // hops[0])
        for way in range(2):
            if step <= hops[way]:
                pass_normed(way, step).wait_recv()
                if step < hops[way]:
                    begin(pass_normed(way, step))
    for m in range(3):
        normed_out[m] = jnp.concatenate(
            [nbuf[j, m].astype(jnp.float32) for j in range(nfs)], axis=0
        ).astype(jnp.bfloat16)
    advance(21)
    fo_copy.wait()
    for copy in stores:
        copy.wait()
    for copy in sends:
        copy.wait_send()


def finish_kernel(f_ref, f_all, normed, weights, gathered, update, new_weights, copies):
    step = jnp.dot(f_ref[...], normed[0], preferred_element_type=jnp.float32)
    update[0] = step
    new_weights[0] = weights[0] - 0.02 * step
    pieces, _, _, half, cols = gathered.shape
    for j in range(pieces):
        step = jnp.dot(f_all[j], normed[0], preferred_element_type=jnp.float32)
        copies[0, j * 2 * half:(j + 1) * 2 * half] = (
            gathered[j, :, 0].astype(jnp.float32).reshape(2 * half, cols) - 0.02 * step
        ).astype(jnp.bfloat16)


def on_device(nfs, ntp, inputs, cotangents, factor, weights, first_moment, second_moment):
    tokens, width = inputs.shape
    held, rank = factor.shape
    rows, cols = first_moment.shape[1:]
    chunk = min(512, tokens)
    chunks = tokens // chunk

    dma = pltpu.SemaphoreType.DMA
    vmem = pl.BlockSpec(memory_space=pltpu.VMEM)
    hbm = pl.BlockSpec(memory_space=pl.ANY)
    new_first, new_second, f_all, normed, gathered = pl.pallas_call(
        functools.partial(exchange_kernel, nfs, ntp, 3 * rank * cols * ntp),
        out_shape=(
            jax.ShapeDtypeStruct(first_moment.shape, jnp.float32),
            jax.ShapeDtypeStruct(second_moment.shape, jnp.float32),
            jax.ShapeDtypeStruct((nfs, 2, held // 2, rank), jnp.bfloat16),
            jax.ShapeDtypeStruct((3, rank, cols), jnp.bfloat16),
            jax.ShapeDtypeStruct((nfs, 2, 3, held // 2, cols), jnp.bfloat16),
        ),
        in_specs=[hbm] * 6,
        out_specs=(vmem, vmem, hbm, vmem, hbm),
        scratch_shapes=[
            pltpu.VMEM((chunks, chunk, width), jnp.bfloat16),
            pltpu.VMEM(cotangents.shape, jnp.bfloat16),
            pltpu.VMEM(weights.shape, jnp.float32),
            pltpu.VMEM(first_moment.shape, jnp.float32),
            pltpu.VMEM(second_moment.shape, jnp.float32),
            pltpu.VMEM((3, rank, cols), jnp.float32),
            pltpu.VMEM((nfs, 2, held // 2, rank), jnp.bfloat16),
            pltpu.VMEM((nfs, 2, 3, held // 2, cols), jnp.bfloat16),
            pltpu.VMEM((nfs, 3, rows, cols), jnp.bfloat16),
            pltpu.VMEM((nfs, 3, rows, cols), jnp.bfloat16),
            pltpu.VMEM((nfs, 3, rows, cols), jnp.bfloat16),
            pltpu.VMEM((1, 128), jnp.float32),
            pltpu.VMEM((ntp, 1, 128), jnp.float32),
            pltpu.VMEM((1, 128), jnp.float32),
            pltpu.VMEM((nfs, 1, 128), jnp.float32),
            dma((chunks,)), dma((3,)), dma((4,)), dma, dma((2, nfs)),
            dma((2, nfs)), dma((nfs,)), dma((2, nfs)), dma((nfs,)),
            dma((2, 3, nfs)), dma((2, 3, nfs)), dma((nfs,)), dma((nfs,)),
            dma((ntp,)), dma((ntp,)), dma((nfs,)), dma((nfs,)), dma((2, nfs)), dma((nfs,)),
        ],
        compiler_params=pltpu.CompilerParams(
            collective_id=0, has_side_effects=True, vmem_limit_bytes=63 * 2**20
        ),
        cost_estimate=pl.CostEstimate(
            flops=50_000_000_000, bytes_accessed=100_000_000, transcendentals=0
        ),
        name="exchange",
    )(
        inputs.reshape(chunks, chunk, width), cotangents,
        factor.reshape(2, held // 2, rank), weights, first_moment, second_moment,
    )
    f_all = f_all.reshape(nfs, held, rank)
    update, new_weights, copies = pl.pallas_call(
        finish_kernel,
        grid=(3,),
        out_shape=(
            jax.ShapeDtypeStruct(weights.shape, jnp.float32),
            jax.ShapeDtypeStruct(weights.shape, jnp.float32),
            jax.ShapeDtypeStruct((3, nfs * held, cols), jnp.bfloat16),
        ),
        in_specs=[
            pl.BlockSpec((held, rank), lambda m: (0, 0)),
            pl.BlockSpec((nfs, held, rank), lambda m: (0, 0, 0)),
            pl.BlockSpec((1, rank, cols), lambda m: (m, 0, 0)),
            pl.BlockSpec((1, held, cols), lambda m: (m, 0, 0)),
            pl.BlockSpec((nfs, 2, 1, held // 2, cols), lambda m: (0, 0, m, 0, 0)),
        ],
        out_specs=(
            pl.BlockSpec((1, held, cols), lambda m: (m, 0, 0)),
            pl.BlockSpec((1, held, cols), lambda m: (m, 0, 0)),
            pl.BlockSpec((1, nfs * held, cols), lambda m: (m, 0, 0)),
        ),
        name="finish",
    )(factor, f_all, normed, weights, gathered)
    return (update, new_weights, copies, new_first, new_second)


def solution(mesh):
    placed = (
        P("fs", None),
        P(None, "fs", "tp"),
        P("fs", None),
        P(None, "fs", "tp"),
        P(None, "fs", "tp"),
        P(None, "fs", "tp"),
    )
    return jax.shard_map(
        functools.partial(on_device, mesh.shape["fs"], mesh.shape["tp"]),
        mesh=mesh,
        in_specs=placed,
        out_specs=(
            P(None, "fs", "tp"),
            P(None, "fs", "tp"),
            P(None, None, "tp"),
            P(None, "fs", "tp"),
            P(None, "fs", "tp"),
        ),
        check_vma=False,
    )
```

time: 101 us -> 74.3 us (0.74)
  between operations: 14.1 us -> 0.66 us
  waiting for transfers between devices: 8.63 us -> 0 us
  Pallas kernels: 74.5 us -> 72.1 us
  other arithmetic: 1.92 us -> 0 us
    all_gather x1 -> x0, waiting for transfers between devices: 8.61 us -> none  [on_device(): gathered = lax.all_gather(weights.astype(jnp.bfloat16), 'fs', axis=0)]
    pallas_call x1, Pallas kernels: 68.5 us -> 66.1 us  [on_device(): pl.pallas_call(functools.partial(exchange_kernel, nfs, ntp, 3 * rank * co...]
    convert_element_type x1 -> x0, other arithmetic: 1.92 us -> none  [on_device(): gathered = lax.all_gather(weights.astype(jnp.bfloat16), 'fs', axis=0)]
  transfers between devices with their start and end apart: 1 -> 0, of which waited for: 1 -> 0; matrix products, arithmetic and copies ran while one was open for 0% -> 0% of each run, Pallas kernels for 68% -> 0%
where the time goes in v2:
time: 74.3 us; the launch traced here: 74.1 us
  Pallas kernels  72.1 us (97%)
  local copies, waits for them, and re-layouts  1.29 us (2%)
    pallas_call x1, Pallas kernels, on_device(): pl.pallas_call(functools.partial(exchange_kernel, nfs, ntp, 3 * rank * co...  66.1 us
    pallas_call x1, Pallas kernels, on_device(): pl.pallas_call(finish_kernel, grid=(3,), out_shape=(jax.ShapeDtypeStruct(...  6.09 us

profile of v2, /device:TPU:0, one launch (start us, length us, event | category | flops | bytes accessed | tf_op | source)
XLA Modules:
  0.0 74.1 jit_solution(7487472088748352788)
XLA Ops:
  0.6 66.1 %exchange.1 = (f32[3,32,256]{2,1,0:T(8,128)}, f32[3,32,256]{2,1,0:T(8,128)}, bf16[8,2,128,256]{3,2,1,0:T(8,128)(2,1)}, bf16[3,256,256]{2,1,0:T(8,128)(2,1)}, bf16[8,2,3,128,256]{4,3,2,1,0:T(8,128)(2,1)}) custom-call(bf16[4,512,2048]{2,1,0:T(8,128)(2,1)} %bitcast.5, bf16[3,2048,256]{2,1,0:T(8,128)(2,1)} %c_hbm.1, bf16[2,128,256]{2,1,0:T(8,128)(2,1)} %bitcast.4, ...), custom_call_target="tpu_custom_call" | custom-call | flops 49999998976 | bytes 100000000 | tf_op jit(solution)/shard_map/exchange/pallas_call | solution.py:263
  66.7 0.0 copy-start.1
  66.7 0.0 copy-start
  66.7 6.1 %finish.1 = (f32[3,256,256]{2,1,0:T(8,128)}, f32[3,256,256]{2,1,0:T(8,128)}, bf16[3,2048,256]{2,1,0:T(8,128)(2,1)}) custom-call(bf16[256,256]{1,0:T(8,128)(2,1)} %f_ref.1, bf16[8,256,256]{2,1,0:T(8,128)(2,1)} %bitcast.3, bf16[3,256,256]{2,1,0:T(8,128)(2,1)} %get-tuple-element.14.normed, f32[3,256,256]{2,1,0:T(8,128)} %weights.1, ...), custom_call_target="tpu_custom_call" | custom-call | tf_op jit(solution)/shard_map/finish/pallas_call | solution.py:307
  72.8 0.0 copy-done.1
  72.8 0.6 copy.13
  73.4 0.0 copy-done
  73.5 0.6 copy.14
Async XLA Ops:
  66.7 6.1 %copy-start.1 = (f32[3,32,256]{2,1,0:T(8,128)S(1)}, f32[3,32,256]{2,1,0:T(8,128)}, u32[]{:S(2)}) copy-start(f32[3,32,256]{2,1,0:T(8,128)} %get-tuple-element.29) | copy-start | bytes 294916
  66.7 6.7 %copy-start = (f32[3,32,256]{2,1,0:T(8,128)S(1)}, f32[3,32,256]{2,1,0:T(8,128)}, u32[]{:S(2)}) copy-start(f32[3,32,256]{2,1,0:T(8,128)} %get-tuple-element.30) | copy-start | bytes 294916

commit v3 on v2

--- a/solution.py
+++ b/solution.py
@@ -131,6 +131,10 @@
 
     for way in range(2):
         begin(pass_factor(way, 0))
+    for way in range(2):
+        for m in range(3):
+            begin(pass_weights(way, 0, m))
+        store_weights(way, 0)
     for step in range(1, hops[0] + 1):
         for way in range(2):
             if step <= hops[way]:
@@ -138,11 +142,7 @@
                 if step < hops[way]:
                     begin(pass_factor(way, step))
                 begin(share_factor(way, step, core))
-        if step <= 3:
-            for way in range(2):
-                begin(pass_weights(way, 0, step - 1))
-                if step == 3:
-                    store_weights(way, 0)
+        advance((step - 1) * 5 // 3)
     for copy in x_copies + c_copies:
         copy.wait()
     for way in range(2):
@@ -162,16 +162,16 @@
                 preferred_element_type=jnp.float32,
             )
         if i < chunks - 1:
-            advance(i + 1)
+            advance(5 + i)
 
     for m in range(3):
         for j in range(nfs):
             pbuf[j, m] = pacc[m, j * rows:(j + 1) * rows, :].astype(jnp.bfloat16)
-    for o, peer in enumerate(peers):
+    for o, peer in reversed(list(enumerate(peers))):
         begin(remote(pbuf.at[peer], rbuf.at[me], p_send.at[o], p_recv.at[me], peer, col))
     projected = pacc[:, pl.ds(pl.multiple_of(me * rows, rows), rows), :]
     for o, peer in enumerate(peers):
-        advance(4 + (o * 6) // len(peers))
+        advance(8 + (o * 3) // len(peers))
         remote(
             pbuf.at[peer], rbuf.at[peer], p_send.at[o], p_recv.at[peer], peer, col
         ).wait_recv()
@@ -186,7 +186,7 @@
     sq_tp[col] = own
     for o, side in enumerate(sides):
         begin(remote(sq_own, sq_tp.at[col], t_send.at[o], t_recv.at[col], me, side))
-    advance(11)
+    advance(12)
     for o, side in enumerate(sides):
         remote(sq_own, sq_tp.at[side], t_send.at[o], t_recv.at[side], me, side).wait_recv()
     mid = jnp.sum(sq_tp[...], axis=0)
@@ -196,7 +196,7 @@
         begin(remote(sq_mid, sq_fs.at[me], s_send.at[o], s_recv.at[me], peer, col))
     for copy in moments:
         copy.wait()
-    advance(13)
+    advance(14)
     for o, peer in enumerate(peers):
         remote(sq_mid, sq_fs.at[peer], s_send.at[o], s_recv.at[peer], peer, col).wait_recv()
     square_sum = jnp.sum(sq_fs[...], axis=0)[:, :1]
@@ -220,7 +220,7 @@
     first_ref[...] = new_first
     second_ref[...] = new_second
     for step in range(1, hops[0] + 1):
-        advance(13 + (step * 7) // hops[0])
+        advance(14 + (step * 7) // hops[0])
         for way in range(2):
             if step <= hops[way]:
                 pass_normed(way, step).wait_recv()
@@ -238,7 +238,12 @@
         copy.wait_send()
 
 
-def finish_kernel(f_ref, f_all, normed, weights, gathered, update, new_weights, copies):
+def finish_kernel(
+    f_ref, f_all, normed, weights, gathered, first, second,
+    update, new_weights, copies, first_out, second_out,
+):
+    first_out[...] = first[...]
+    second_out[...] = second[...]
     step = jnp.dot(f_ref[...], normed[0], preferred_element_type=jnp.float32)
     update[0] = step
     new_weights[0] = weights[0] - 0.02 * step
@@ -304,13 +309,15 @@
         factor.reshape(2, held // 2, rank), weights, first_moment, second_moment,
     )
     f_all = f_all.reshape(nfs, held, rank)
-    update, new_weights, copies = pl.pallas_call(
+    update, new_weights, copies, new_first, new_second = pl.pallas_call(
         finish_kernel,
         grid=(3,),
         out_shape=(
             jax.ShapeDtypeStruct(weights.shape, jnp.float32),
             jax.ShapeDtypeStruct(weights.shape, jnp.float32),
             jax.ShapeDtypeStruct((3, nfs * held, cols), jnp.bfloat16),
+            jax.ShapeDtypeStruct(first_moment.shape, jnp.float32),
+            jax.ShapeDtypeStruct(second_moment.shape, jnp.float32),
         ),
         in_specs=[
             pl.BlockSpec((held, rank), lambda m: (0, 0)),
@@ -318,14 +325,18 @@
             pl.BlockSpec((1, rank, cols), lambda m: (m, 0, 0)),
             pl.BlockSpec((1, held, cols), lambda m: (m, 0, 0)),
             pl.BlockSpec((nfs, 2, 1, held // 2, cols), lambda m: (0, 0, m, 0, 0)),
+            pl.BlockSpec((1, rows, cols), lambda m: (m, 0, 0)),
+            pl.BlockSpec((1, rows, cols), lambda m: (m, 0, 0)),
         ],
         out_specs=(
             pl.BlockSpec((1, held, cols), lambda m: (m, 0, 0)),
             pl.BlockSpec((1, held, cols), lambda m: (m, 0, 0)),
             pl.BlockSpec((1, nfs * held, cols), lambda m: (m, 0, 0)),
+            pl.BlockSpec((1, rows, cols), lambda m: (m, 0, 0)),
+            pl.BlockSpec((1, rows, cols), lambda m: (m, 0, 0)),
         ),
         name="finish",
-    )(factor, f_all, normed, weights, gathered)
+    )(factor, f_all, normed, weights, gathered, new_first, new_second)
     return (update, new_weights, copies, new_first, new_second)
 
 

time: 74.3 us -> 71.1 us (0.957)
  Pallas kernels: 72.1 us -> 70.2 us
  local copies, waits for them, and re-layouts: 1.29 us -> 0 us
    pallas_call x1, Pallas kernels: 66.1 us -> 64.1 us  [on_device(): pl.pallas_call(functools.partial(exchange_kernel, nfs, ntp, 3 * rank * co...]
    unnamed x6 -> x0, local copies, waits for them, and re-layouts: 1.29 us -> none
where the time goes in v3:
time: 71.1 us; the launch traced here: 70.9 us
  Pallas kernels  70.2 us (99%)
    pallas_call x1, Pallas kernels, on_device(): pl.pallas_call(functools.partial(exchange_kernel, nfs, ntp, 3 * rank * co...  64.1 us
    pallas_call x1, Pallas kernels, on_device(): pl.pallas_call(finish_kernel, grid=(3,), out_shape=(jax.ShapeDtypeStruct(...  6.19 us

profile of v3, /device:TPU:0, one launch (start us, length us, event | category | flops | bytes accessed | tf_op | source)
XLA Modules:
  0.0 70.9 jit_solution(15932281067253386105)
XLA Ops:
  0.6 64.1 %exchange.1 = (f32[3,32,256]{2,1,0:T(8,128)}, f32[3,32,256]{2,1,0:T(8,128)}, bf16[8,2,128,256]{3,2,1,0:T(8,128)(2,1)}, bf16[3,256,256]{2,1,0:T(8,128)(2,1)}, bf16[8,2,3,128,256]{4,3,2,1,0:T(8,128)(2,1)}) custom-call(bf16[4,512,2048]{2,1,0:T(8,128)(2,1)} %bitcast.5, bf16[3,2048,256]{2,1,0:T(8,128)(2,1)} %c_hbm.1, bf16[2,128,256]{2,1,0:T(8,128)(2,1)} %bitcast.4, ...), custom_call_target="tpu_custom_call" | custom-call | flops 49999998976 | bytes 100000000 | tf_op jit(solution)/shard_map/exchange/pallas_call | solution.py:268
  64.7 6.2 %finish.1 = (f32[3,256,256]{2,1,0:T(8,128)}, f32[3,256,256]{2,1,0:T(8,128)}, bf16[3,2048,256]{2,1,0:T(8,128)(2,1)}, f32[3,32,256]{2,1,0:T(8,128)}, f32[3,32,256]{2,1,0:T(8,128)}) custom-call(bf16[256,256]{1,0:T(8,128)(2,1)} %f_ref.1, bf16[8,256,256]{2,1,0:T(8,128)(2,1)} %bitcast.3, bf16[3,256,256]{2,1,0:T(8,128)(2,1)} %get-tuple-element.11.normed, ...), custom_call_target="tpu_custom_call" | custom-call | tf_op jit(solution)/shard_map/finish/pallas_call | solution.py:312
